TPU v7x, 32 devices: a whole 2x2x4 slice. The times are simulated.
32 devices in a mesh: fs: 4 (over z), rep: 4 (over y, x), tp: 2 (over core).
Axes of the slice: x: 2, y: 2, z: 4, core: 2. Of those that a mesh axis runs over, the one named last changes fastest.
Arguments:
- mixer_input: bfloat16 [32768, 2048], P(('fs', 'rep')), may hold values from -6 to 6
- value_cot: bfloat16 [32768, 2048], P(('fs', 'rep'), 'tp'), may hold values from -0.22097087 to 0.22097087
- gate_cot: bfloat16 [32768, 2048], P(('fs', 'rep'), 'tp'), may hold values from -0.22097087 to 0.22097087
- value_weight: float32 [2048, 2048], P('fs', 'tp'), may hold values from -0.125 to 0.125
- gate_weight: float32 [2048, 2048], P('fs', 'tp'), may hold values from -0.125 to 0.125
- value_basis: bfloat16 [2048, 256], replicated, may hold values from -0.8838835 to 0.8838835
- gate_basis: bfloat16 [2048, 256], replicated, may hold values from -0.8838835 to 0.8838835
- value_first: float32 [256, 2048], P('fs', 'tp'), may hold values from -6 to 6
- gate_first: float32 [256, 2048], P('fs', 'tp'), may hold values from -6 to 6
- value_second: float32 [256, 2048], P('fs', 'tp'), may hold values from 0.01 to 1
- gate_second: float32 [256, 2048], P('fs', 'tp'), may hold values from 0.01 to 1
Outputs:
- value_new: float32 [2048, 2048], P('fs', 'tp')
- gate_new: float32 [2048, 2048], P('fs', 'tp')
- value_copy: bfloat16 [2048, 2048], P(None, 'tp')
- gate_copy: bfloat16 [2048, 2048], P(None, 'tp')
- value_step: float32 [2048, 2048], P('fs', 'tp')
- gate_step: float32 [2048, 2048], P('fs', 'tp')
- value_first_new: float32 [256, 2048], P('fs', 'tp')
- gate_first_new: float32 [256, 2048], P('fs', 'tp')
- value_second_new: float32 [256, 2048], P('fs', 'tp')
- gate_second_new: float32 [256, 2048], P('fs', 'tp')
All inputs are finite; a program needn't handle non-finite values.
Results may differ from a plain program's by a relative error of at most 0.0044.
Values may be sent and summed in bfloat16 or wider, within the bound.
A program may use at most 128 MiB of HBM per device.

v0:
```python
import jax
import jax.numpy as jnp
from jax import lax
from jax.sharding import PartitionSpec as P

D = 2048
learn_rate = 0.02


def local(
    mixer_input,
    value_cot,
    gate_cot,
    value_weight,
    gate_weight,
    value_basis,
    gate_basis,
    value_first,
    gate_first,
    value_second,
    gate_second,
):
    half_cols = value_cot.shape[1]
    rows_dev = value_weight.shape[0]
    fs_index = lax.axis_index("fs")
    own_value = lax.dynamic_slice_in_dim(value_basis, fs_index * rows_dev, rows_dev, 0)
    own_gate = lax.dynamic_slice_in_dim(gate_basis, fs_index * rows_dev, rows_dev, 0)
    value_proj = jnp.dot(mixer_input, value_basis, preferred_element_type=jnp.float32)
    gate_proj = jnp.dot(mixer_input, gate_basis, preferred_element_type=jnp.float32)
    upper_value = lax.optimization_barrier(value_proj.astype(jnp.bfloat16))
    upper_gate = lax.optimization_barrier(gate_proj.astype(jnp.bfloat16))
    lower_value = (value_proj - upper_value.astype(jnp.float32)).astype(jnp.bfloat16)
    lower_gate = (gate_proj - upper_gate.astype(jnp.float32)).astype(jnp.bfloat16)
    value_part = jnp.dot(upper_value.T, value_cot, preferred_element_type=jnp.float32) + jnp.dot(
        lower_value.T, value_cot, preferred_element_type=jnp.float32
    )
    gate_part = jnp.dot(upper_gate.T, gate_cot, preferred_element_type=jnp.float32) + jnp.dot(
        lower_gate.T, gate_cot, preferred_element_type=jnp.float32
    )
    partial_value = lax.psum_scatter(
        jnp.concatenate([value_part, gate_part], axis=1), "fs", scatter_dimension=0, tiled=True
    )
    projected = lax.psum(partial_value, "rep")
    value_small = projected[:, :half_cols]
    gate_small = projected[:, half_cols:]
    value_first_new = 0.9 * value_first + 0.1 * value_small
    gate_first_new = 0.9 * gate_first + 0.1 * gate_small
    value_second_new = 0.95 * value_second + 0.05 * value_small * value_small
    gate_second_new = 0.95 * gate_second + 0.05 * gate_small * gate_small
    scaled = jnp.concatenate(
        [
            value_first_new * lax.rsqrt(value_second_new),
            gate_first_new * lax.rsqrt(gate_second_new),
        ],
        axis=1,
    ).astype(jnp.bfloat16)
    piece = lax.all_gather(scaled, "fs", axis=0, tiled=True)
    value_part = jnp.dot(own_value, piece[:, :half_cols], preferred_element_type=jnp.float32)
    gate_part = jnp.dot(own_gate, piece[:, half_cols:], preferred_element_type=jnp.float32)
    expanded = jnp.concatenate([value_part, gate_part], axis=1)
    value_full = expanded[:, :half_cols]
    gate_full = expanded[:, half_cols:]
    squares = lax.psum(
        (jnp.sum(value_full * value_full), jnp.sum(gate_full * gate_full)), ("fs", "tp")
    )
    entries = float(D * D)
    value_step = value_full * lax.rsqrt(squares[0] / entries + 1e-06)
    gate_step = gate_full * lax.rsqrt(squares[1] / entries + 1e-06)
    value_new = value_weight - learn_rate * value_step
    gate_new = gate_weight - learn_rate * gate_step
    copies = (
        lax.all_gather(value_new.astype(jnp.bfloat16), "fs", axis=0, tiled=True),
        lax.all_gather(gate_new.astype(jnp.bfloat16), "fs", axis=0, tiled=True),
    )
    return (
        value_new,
        gate_new,
        copies[0],
        copies[1],
        value_step,
        gate_step,
        value_first_new,
        gate_first_new,
        value_second_new,
        gate_second_new,
    )


def solution(mesh):
    return jax.shard_map(
        local,
        mesh=mesh,
        in_specs=(
            P(("fs", "rep"), None),
            P(("fs", "rep"), "tp"),
            P(("fs", "rep"), "tp"),
            P("fs", "tp"),
            P("fs", "tp"),
            P(),
            P(),
            P("fs", "tp"),
            P("fs", "tp"),
            P("fs", "tp"),
            P("fs", "tp"),
        ),
        out_specs=(
            P("fs", "tp"),
            P("fs", "tp"),
            P(None, "tp"),
            P(None, "tp"),
            P("fs", "tp"),
            P("fs", "tp"),
            P("fs", "tp"),
            P("fs", "tp"),
            P("fs", "tp"),
            P("fs", "tp"),
        ),
        check_vma=False,
    )
```

profile of v0, /device:TPU:0, one launch (start us, length us, event | category | flops | bytes accessed | tf_op | source)
XLA Modules:
  0.0 350.1 jit_solution(15234940572082400259)
XLA Ops:
  7.2 0.0 copy-start
  7.2 0.0 reduce-scatter.2.cloned.1.call-start
  7.2 0.0 copy-start.9
  7.2 6.2 %fusion.15 = (bf16[2048,256]{1,0:T(8,128)(2,1)S(1)}, f32[2048,256]{1,0:T(8,128)S(1)}) fusion(bf16[2048,2048]{1,0:T(8,128)(2,1)} %param.11, bf16[2048,256]{1,0:T(8,128)(2,1)} %param.16), kind=kOutput, calls=%fused_computation.31 | convolution fusion | flops 2148007936 | bytes 12582912 | tf_op jit(solution)/shard_map/dot_general | solution.py:28
  13.5 0.0 copy-done
  13.5 0.1 copy-done.9
  13.6 0.0 copy-start.1
  13.6 2.4 fusion.14
  16.0 0.0 copy-done.1
  16.1 1.3 fusion.16
  17.3 0.0 copy-start.2
  17.3 1.3 convolution_add_fusion.1
  18.6 0.9 copy-done.2
  19.5 1.3 fusion.17
  20.8 1.3 convolution_add_fusion
  22.1 1.5 pad_maximum_fusion
  23.5 0.0 copy-start.5
  23.5 0.0 copy-start.6
  23.5 0.0 copy-start.7
  23.6 0.0 copy-start.8
  23.6 0.0 reduce-scatter.2.cloned.1.call-update
  23.6 0.0 all-reduce.3.cloned.1.call-start
  23.6 46.5 %reduce-scatter.2.cloned.1.call-done = f32[64,2048]{1,0:T(8,128)} async-done(((f32[256,2048]{1,0:T(8,128)}), f32[64,2048]{1,0:T(8,128)}) %reduce-scatter.2.cloned.1.call-update) | async-done | bytes 524304 | tf_op jit(solution)/shard_map/reduce_scatter | solution.py:40
  70.1 0.0 all-reduce.3.cloned.1.call-update
  70.1 0.0 all-gather.4.cloned.1.call-start
  70.2 47.5 %all-reduce.3.cloned.1.call-done = f32[64,2048]{1,0:T(8,128)} async-done(((f32[64,2048]{1,0:T(8,128)}), f32[64,2048]{1,0:T(8,128)}) %all-reduce.3.cloned.1.call-update) | async-done | bytes 524304 | tf_op jit(solution)/shard_map/psum | solution.py:43
  117.7 0.0 copy-done.5
  117.7 0.0 copy-done.6
  117.7 0.0 copy-done.7
  117.7 0.0 copy-done.8
  117.7 2.1 multiply_convert_fusion.1
  119.8 0.7 pad_maximum_fusion.1
  120.5 0.0 all-gather.4.cloned.1.call-update
  120.5 0.0 all-gather.6.cloned.1.call-start
  120.6 28.1 %all-gather.4.cloned.1.call-done = bf16[256,2048]{1,0:T(8,128)(2,1)} async-done(((bf16[64,2048]{1,0:T(8,128)(2,1)}), bf16[256,2048]{1,0:T(8,128)(2,1)}) %all-gather.4.cloned.1.call-update) | async-done | bytes 1048592 | tf_op jit(solution)/shard_map/all_gather | solution.py:57
  148.7 0.0 copy-start.4
  148.7 2.4 multiply_reduce_fusion
  151.1 0.0 copy-done.4
  151.1 3.5 multiply_reduce_fusion.1
  154.6 15.3 %all-reduce = (f32[]{:T(128)}, f32[]{:T(128)}) all-reduce(f32[]{:T(128)} %get-tuple-element.31, f32[]{:T(128)} %get-tuple-element.33), channel_id=1, replica_groups=mesh['fs'=4,'rep'=4,'tp'=2] {'fs','tp'}, use_global_device_ids=true, to_apply=%region_3.0 | all-reduce | flops 2 | bytes 16 | tf_op jit(solution)/shard_map/psum | solution.py:63
  170.6 5.6 %fusion.11 = (bf16[512,1024]{1,0:T(8,128)(2,1)}, f32[512,1024]{1,0:T(8,128)}, f32[512,1024]{1,0:T(8,128)}) fusion(f32[512,1024]{1,0:T(8,128)} %param.14, f32[512,1024]{1,0:T(8,128)} %get-tuple-element.32, f32[]{:T(128)S(6)} %rsqrt.14), kind=kLoop, calls=%fused_computation.29 | loop fusion | flops 2097152 | bytes 9437188 | tf_op jit(solution)/shard_map/convert_element_type | solution.py:72
  176.2 0.0 all-gather.6.cloned.1.call-update
  176.2 0.0 all-gather.8.cloned.1.call-start
  177.0 4.8 %fusion.10 = (bf16[512,1024]{1,0:T(8,128)(2,1)}, f32[512,1024]{1,0:T(8,128)}, f32[512,1024]{1,0:T(8,128)}) fusion(f32[512,1024]{1,0:T(8,128)} %param.15, f32[512,1024]{1,0:T(8,128)S(1)} %get-tuple-element.34, f32[]{:T(128)S(6)} %rsqrt.15), kind=kLoop, calls=%fused_computation.28 | loop fusion | flops 2097152 | bytes 9437188 | tf_op jit(solution)/shard_map/convert_element_type | solution.py:73
  181.7 0.0 all-gather.8.cloned.1.call-update
  181.7 73.7 %all-gather.6.cloned.1.call-done = bf16[2048,1024]{1,0:T(8,128)(2,1)} async-done(((bf16[512,1024]{1,0:T(8,128)(2,1)}), bf16[2048,1024]{1,0:T(8,128)(2,1)}) %all-gather.6.cloned.1.call-update) | async-done | bytes 4194320 | tf_op jit(solution)/shard_map/all_gather | solution.py:72
  255.5 81.2 %all-gather.8.cloned.1.call-done = bf16[2048,1024]{1,0:T(8,128)(2,1)} async-done(((bf16[512,1024]{1,0:T(8,128)(2,1)}), bf16[2048,1024]{1,0:T(8,128)(2,1)}) %all-gather.8.cloned.1.call-update) | async-done | bytes 4194320 | tf_op jit(solution)/shard_map/all_gather | solution.py:73
  336.7 0.0 copy-start.3
  336.7 4.8 %copy.24 = bf16[2048,1024]{1,0:T(8,128)(2,1)} copy(bf16[2048,1024]{1,0:T(8,128)(2,1)} %all-gather.6.cloned.1.call-done) | data formatting | bytes 8388608
  341.5 0.0 copy-done.3
  341.5 2.0 copy.25
Async XLA Ops:
  7.2 6.3 %copy-start = (bf16[2048,256]{1,0:T(8,128)(2,1)S(1)}, bf16[2048,256]{1,0:T(8,128)(2,1)}, u32[]{:S(2)}) copy-start(bf16[2048,256]{1,0:T(8,128)(2,1)} %param.17) | copy-start | bytes 3145732
  7.2 62.9 %reduce-scatter.2.cloned.1.call-start = ((), (), s32[]{:S(2)}) async-start(), calls=%async_computation.1 | async-start | bytes 2621440 | tf_op jit(solution)/shard_map/reduce_scatter | solution.py:40
  7.2 6.4 %copy-start.9 = (bf16[2048,2048]{1,0:T(8,128)(2,1)S(1)}, bf16[2048,2048]{1,0:T(8,128)(2,1)}, u32[]{:S(2)}) copy-start(bf16[2048,2048]{1,0:T(8,128)(2,1)} %param.11) | copy-start | bytes 25165828
  13.6 2.4 copy-start.1
  17.3 2.2 copy-start.2
  23.5 94.1 %copy-start.5 = (f32[64,1024]{1,0:T(8,128)S(1)}, f32[64,1024]{1,0:T(8,128)}, u32[]{:S(2)}) copy-start(f32[64,1024]{1,0:T(8,128)} %param.20) | copy-start | bytes 786436
  23.5 94.1 %copy-start.6 = (f32[64,1024]{1,0:T(8,128)S(1)}, f32[64,1024]{1,0:T(8,128)}, u32[]{:S(2)}) copy-start(f32[64,1024]{1,0:T(8,128)} %param.18) | copy-start | bytes 786436
  23.5 94.1 %copy-start.7 = (f32[64,1024]{1,0:T(8,128)S(1)}, f32[64,1024]{1,0:T(8,128)}, u32[]{:S(2)}) copy-start(f32[64,1024]{1,0:T(8,128)} %param.21) | copy-start | bytes 786436
  23.6 94.1 %copy-start.8 = (f32[64,1024]{1,0:T(8,128)S(1)}, f32[64,1024]{1,0:T(8,128)}, u32[]{:S(2)}) copy-start(f32[64,1024]{1,0:T(8,128)} %param.19) | copy-start | bytes 786436
  23.6 94.1 %all-reduce.3.cloned.1.call-start = ((), (), s32[]{:S(2)}) async-start(), calls=%async_computation.2 | async-start | bytes 1048576 | tf_op jit(solution)/shard_map/psum | solution.py:43
  70.1 78.6 %all-gather.4.cloned.1.call-start = ((), (), s32[]{:S(2)}) async-start(), calls=%async_computation.3 | async-start | bytes 1310720 | tf_op jit(solution)/shard_map/all_gather | solution.py:57
  120.5 134.9 %all-gather.6.cloned.1.call-start = ((), (), s32[]{:S(2)}) async-start(), calls=%async_computation.4 | async-start | bytes 5242880 | tf_op jit(solution)/shard_map/all_gather | solution.py:72
  148.7 2.4 copy-start.4
  176.2 160.5 %all-gather.8.cloned.1.call-start = ((), (), s32[]{:S(2)}) async-start(), calls=%async_computation.5 | async-start | bytes 5242880 | tf_op jit(solution)/shard_map/all_gather | solution.py:73
  336.7 4.8 %copy-start.3 = (bf16[2048,1024]{1,0:T(8,128)(2,1)S(1)}, bf16[2048,1024]{1,0:T(8,128)(2,1)}, u32[]{:S(2)}) copy-start(bf16[2048,1024]{1,0:T(8,128)(2,1)} %all-gather.8.cloned.1.call-done) | copy-start | bytes 12582916
Sparse Core Ops, SparseCore 0:
  23.7 46.3 reduce-scatter.1
  73.1 44.5 all-reduce.2
  120.7 27.9 all-gather.3
  176.3 79.0 all-gather.5
  257.5 79.2 all-gather.7
where the time goes:
time: 350 us
  waiting for transfers between devices  277 us (79%)
  matrix products  19.7 us (6%)
  blocking collectives  15.3 us (4%)
  between operations  15.3 us (4%)
  other arithmetic  14.6 us (4%)
  local copies, waits for them, and re-layouts  7.86 us (2%)
    all_gather x1, waiting for transfers between devices, local(): lax.all_gather(gate_new.astype(jnp.bfloat16), 'fs', axis=0, tiled=True)  81.2 us
    all_gather x1, waiting for transfers between devices, local(): lax.all_gather(value_new.astype(jnp.bfloat16), 'fs', axis=0, tiled=True)  73.7 us
    psum x1, waiting for transfers between devices, local(): projected = lax.psum(partial_value, 'rep')  47.5 us
    reduce_scatter x1, waiting for transfers between devices, local(): lax.psum_scatter(jnp.concatenate([value_part, gate_part], axis=1), 'fs',...  46.5 us
    all_gather x1, waiting for transfers between devices, local(): piece = lax.all_gather(scaled, 'fs', axis=0, tiled=True)  28.1 us
    psum x1, blocking collectives, local(): lax.psum((jnp.sum(value_full * value_full), jnp.sum(gate_full * gate_full...  15.3 us
    unnamed x22, local copies, waits for them, and re-layouts  7.86 us
  transfers between devices with their start and end apart: 5, of which 5 were waited for; matrix products, arithmetic and copies ran while one was open for 1% of the time, Pallas kernels for 0%

commit v1 on v0

--- a/solution.py
+++ b/solution.py
@@ -40,7 +40,7 @@
     partial_value = lax.psum_scatter(
         jnp.concatenate([value_part, gate_part], axis=1), "fs", scatter_dimension=0, tiled=True
     )
-    projected = lax.psum(partial_value, "rep")
+    projected = jnp.sum(lax.all_gather(partial_value, "rep"), axis=0)
     value_small = projected[:, :half_cols]
     gate_small = projected[:, half_cols:]
     value_first_new = 0.9 * value_first + 0.1 * value_small

time: 350 us -> 340 us (0.971)
  waiting for transfers between devices: 277 us -> 266 us
    psum x1 -> x0, waiting for transfers between devices: 47.5 us -> none  [local(): projected = lax.psum(partial_value, 'rep')]
    all_gather x0 -> x1, waiting for transfers between devices: none -> 36.2 us  [local(): projected = jnp.sum(lax.all_gather(partial_value, 'rep'), axis=0)]
where the time goes in v1:
time: 340 us; the launch traced here: 339 us
  waiting for transfers between devices  266 us (78%)
  matrix products  19.7 us (6%)
  other arithmetic  15.4 us (5%)
  blocking collectives  15.3 us (4%)
  between operations  15.3 us (4%)
  local copies, waits for them, and re-layouts  7.87 us (2%)
    all_gather x1, waiting for transfers between devices, local(): lax.all_gather(gate_new.astype(jnp.bfloat16), 'fs', axis=0, tiled=True)  81.2 us
    all_gather x1, waiting for transfers between devices, local(): lax.all_gather(value_new.astype(jnp.bfloat16), 'fs', axis=0, tiled=True)  73.7 us
    reduce_scatter x1, waiting for transfers between devices, local(): lax.psum_scatter(jnp.concatenate([value_part, gate_part], axis=1), 'fs',...  46.4 us
    all_gather x1, waiting for transfers between devices, local(): projected = jnp.sum(lax.all_gather(partial_value, 'rep'), axis=0)  36.2 us
    all_gather x1, waiting for transfers between devices, local(): piece = lax.all_gather(scaled, 'fs', axis=0, tiled=True)  28.1 us
    psum x1, blocking collectives, local(): lax.psum((jnp.sum(value_full * value_full), jnp.sum(gate_full * gate_full...  15.3 us
    unnamed x22, local copies, waits for them, and re-layouts  7.87 us
  transfers between devices with their start and end apart: 5, of which 5 were waited for; matrix products, arithmetic and copies ran while one was open for 1% of the time, Pallas kernels for 0%

profile of v1, /device:TPU:0, one launch (start us, length us, event | category | flops | bytes accessed | tf_op | source)
XLA Modules:
  0.0 339.5 jit_solution(10073231918362812263)
XLA Ops:
  7.2 0.0 copy-start
  7.2 0.0 reduce-scatter.2.cloned.1.call-start
  7.2 0.0 copy-start.9
  7.2 6.2 %fusion.15 = (bf16[2048,256]{1,0:T(8,128)(2,1)S(1)}, f32[2048,256]{1,0:T(8,128)S(1)}) fusion(bf16[2048,2048]{1,0:T(8,128)(2,1)} %param.11, bf16[2048,256]{1,0:T(8,128)(2,1)} %param.16), kind=kOutput, calls=%fused_computation.31 | convolution fusion | flops 2148007936 | bytes 12582912 | tf_op jit(solution)/shard_map/dot_general | solution.py:28
  13.5 0.0 copy-done
  13.5 0.1 copy-done.9
  13.6 0.0 copy-start.1
  13.6 2.4 fusion.14
  16.0 0.0 copy-done.1
  16.1 1.3 fusion.16
  17.3 0.0 copy-start.2
  17.3 1.3 convolution_add_fusion.1
  18.6 0.9 copy-done.2
  19.5 1.3 fusion.17
  20.8 1.3 convolution_add_fusion
  22.1 1.5 pad_maximum_fusion
  23.5 0.0 reduce-scatter.2.cloned.1.call-update
  23.6 0.0 copy-start.5
  23.6 0.0 copy-start.6
  23.6 0.0 copy-start.7
  23.6 0.0 copy-start.8
  23.6 0.0 all-gather.12.cloned.1.call-start
  23.7 46.4 %reduce-scatter.2.cloned.1.call-done = f32[64,2048]{1,0:T(8,128)} async-done(((f32[256,2048]{1,0:T(8,128)}), f32[64,2048]{1,0:T(8,128)}) %reduce-scatter.2.cloned.1.call-update) | async-done | bytes 524304 | tf_op jit(solution)/shard_map/reduce_scatter | solution.py:40
  70.1 0.0 all-gather.12.cloned.1.call-update
  70.1 0.0 all-gather.6.cloned.1.call-start
  70.1 36.2 %all-gather.12.cloned.1.call-done = f32[256,2048]{1,0:T(8,128)} async-done(((f32[64,2048]{1,0:T(8,128)}), f32[256,2048]{1,0:T(8,128)}) %all-gather.12.cloned.1.call-update) | async-done | bytes 2097168 | tf_op jit(solution)/shard_map/all_gather | solution.py:43
  106.3 1.8 reduce_sum.27
  108.1 0.0 copy-done.5
  108.1 0.0 copy-done.6
  108.1 0.0 copy-done.7
  108.1 0.0 copy-done.8
  108.1 1.1 multiply_convert_fusion.1
  109.2 0.7 pad_maximum_fusion.1
  109.9 0.0 all-gather.6.cloned.1.call-update
  110.0 0.0 all-gather.8.cloned.1.call-start
  110.0 28.1 %all-gather.6.cloned.1.call-done = bf16[256,2048]{1,0:T(8,128)(2,1)} async-done(((bf16[64,2048]{1,0:T(8,128)(2,1)}), bf16[256,2048]{1,0:T(8,128)(2,1)}) %all-gather.6.cloned.1.call-update) | async-done | bytes 1048592 | tf_op jit(solution)/shard_map/all_gather | solution.py:57
  138.1 0.0 copy-start.4
  138.1 2.4 multiply_reduce_fusion
  140.5 0.0 copy-done.4
  140.5 3.5 %multiply_reduce_fusion.1 = (f32[]{:T(128)}, f32[512,1024]{1,0:T(8,128)}) fusion(bf16[256,2048]{1,0:T(8,128)(2,1)S(1)} %copy-done.4, bf16[2048,256]{1,0:T(8,128)(2,1)} %param.16, s32[]{:T(128)S(6)} %select_n.4), kind=kOutput, calls=%fused_computation.4 | convolution fusion | flops 269484032 | bytes 2883592 | tf_op jit(solution)/shard_map/dot_general | solution.py:58
  144.0 15.3 %all-reduce = (f32[]{:T(128)}, f32[]{:T(128)}) all-reduce(f32[]{:T(128)} %get-tuple-element.31, f32[]{:T(128)} %get-tuple-element.33), channel_id=1, replica_groups=mesh['fs'=4,'rep'=4,'tp'=2] {'fs','tp'}, use_global_device_ids=true, to_apply=%region_3.0 | all-reduce | flops 2 | bytes 16 | tf_op jit(solution)/shard_map/psum | solution.py:63
  160.0 5.6 %fusion.11 = (bf16[512,1024]{1,0:T(8,128)(2,1)}, f32[512,1024]{1,0:T(8,128)}, f32[512,1024]{1,0:T(8,128)}) fusion(f32[512,1024]{1,0:T(8,128)} %param.14, f32[512,1024]{1,0:T(8,128)} %get-tuple-element.32, f32[]{:T(128)S(6)} %rsqrt.14), kind=kLoop, calls=%fused_computation.29 | loop fusion | flops 2097152 | bytes 9437188 | tf_op jit(solution)/shard_map/convert_element_type | solution.py:72
  165.6 0.0 all-gather.8.cloned.1.call-update
  165.6 0.0 all-gather.10.cloned.1.call-start
  166.4 4.8 %fusion.10 = (bf16[512,1024]{1,0:T(8,128)(2,1)}, f32[512,1024]{1,0:T(8,128)}, f32[512,1024]{1,0:T(8,128)}) fusion(f32[512,1024]{1,0:T(8,128)} %param.15, f32[512,1024]{1,0:T(8,128)S(1)} %get-tuple-element.34, f32[]{:T(128)S(6)} %rsqrt.15), kind=kLoop, calls=%fused_computation.28 | loop fusion | flops 2097152 | bytes 9437188 | tf_op jit(solution)/shard_map/convert_element_type | solution.py:73
  171.1 0.0 all-gather.10.cloned.1.call-update
  171.1 73.7 %all-gather.8.cloned.1.call-done = bf16[2048,1024]{1,0:T(8,128)(2,1)} async-done(((bf16[512,1024]{1,0:T(8,128)(2,1)}), bf16[2048,1024]{1,0:T(8,128)(2,1)}) %all-gather.8.cloned.1.call-update) | async-done | bytes 4194320 | tf_op jit(solution)/shard_map/all_gather | solution.py:72
  244.9 81.2 %all-gather.10.cloned.1.call-done = bf16[2048,1024]{1,0:T(8,128)(2,1)} async-done(((bf16[512,1024]{1,0:T(8,128)(2,1)}), bf16[2048,1024]{1,0:T(8,128)(2,1)}) %all-gather.10.cloned.1.call-update) | async-done | bytes 4194320 | tf_op jit(solution)/shard_map/all_gather | solution.py:73
  326.1 0.0 copy-start.3
  326.1 4.8 %copy.23 = bf16[2048,1024]{1,0:T(8,128)(2,1)} copy(bf16[2048,1024]{1,0:T(8,128)(2,1)} %all-gather.8.cloned.1.call-done) | data formatting | bytes 8388608
  330.9 0.0 copy-done.3
  330.9 2.0 copy.24
Async XLA Ops:
  7.2 6.3 %copy-start = (bf16[2048,256]{1,0:T(8,128)(2,1)S(1)}, bf16[2048,256]{1,0:T(8,128)(2,1)}, u32[]{:S(2)}) copy-start(bf16[2048,256]{1,0:T(8,128)(2,1)} %param.17) | copy-start | bytes 3145732
  7.2 62.9 %reduce-scatter.2.cloned.1.call-start = ((), (), s32[]{:S(2)}) async-start(), calls=%async_computation.1 | async-start | bytes 2621440 | tf_op jit(solution)/shard_map/reduce_scatter | solution.py:40
  7.2 6.4 %copy-start.9 = (bf16[2048,2048]{1,0:T(8,128)(2,1)S(1)}, bf16[2048,2048]{1,0:T(8,128)(2,1)}, u32[]{:S(2)}) copy-start(bf16[2048,2048]{1,0:T(8,128)(2,1)} %param.11) | copy-start | bytes 25165828
  13.6 2.4 copy-start.1
  17.3 2.2 copy-start.2
  23.6 84.5 %copy-start.5 = (f32[64,1024]{1,0:T(8,128)S(1)}, f32[64,1024]{1,0:T(8,128)}, u32[]{:S(2)}) copy-start(f32[64,1024]{1,0:T(8,128)} %param.20) | copy-start | bytes 786436
  23.6 84.5 %copy-start.6 = (f32[64,1024]{1,0:T(8,128)S(1)}, f32[64,1024]{1,0:T(8,128)}, u32[]{:S(2)}) copy-start(f32[64,1024]{1,0:T(8,128)} %param.18) | copy-start | bytes 786436
  23.6 84.5 %copy-start.7 = (f32[64,1024]{1,0:T(8,128)S(1)}, f32[64,1024]{1,0:T(8,128)}, u32[]{:S(2)}) copy-start(f32[64,1024]{1,0:T(8,128)} %param.21) | copy-start | bytes 786436
  23.6 84.5 %copy-start.8 = (f32[64,1024]{1,0:T(8,128)S(1)}, f32[64,1024]{1,0:T(8,128)}, u32[]{:S(2)}) copy-start(f32[64,1024]{1,0:T(8,128)} %param.19) | copy-start | bytes 786436
  23.6 82.7 %all-gather.12.cloned.1.call-start = ((), (), s32[]{:S(2)}) async-start(), calls=%async_computation.5 | async-start | bytes 2621440 | tf_op jit(solution)/shard_map/all_gather | solution.py:43
  70.1 68.0 %all-gather.6.cloned.1.call-start = ((), (), s32[]{:S(2)}) async-start(), calls=%async_computation.2 | async-start | bytes 1310720 | tf_op jit(solution)/shard_map/all_gather | solution.py:57
  110.0 134.9 %all-gather.8.cloned.1.call-start = ((), (), s32[]{:S(2)}) async-start(), calls=%async_computation.3 | async-start | bytes 5242880 | tf_op jit(solution)/shard_map/all_gather | solution.py:72
  138.1 2.4 copy-start.4
  165.6 160.5 %all-gather.10.cloned.1.call-start = ((), (), s32[]{:S(2)}) async-start(), calls=%async_computation.4 | async-start | bytes 5242880 | tf_op jit(solution)/shard_map/all_gather | solution.py:73
  326.1 4.8 %copy-start.3 = (bf16[2048,1024]{1,0:T(8,128)(2,1)S(1)}, bf16[2048,1024]{1,0:T(8,128)(2,1)}, u32[]{:S(2)}) copy-start(bf16[2048,1024]{1,0:T(8,128)(2,1)} %all-gather.10.cloned.1.call-done) | copy-start | bytes 12582916
Sparse Core Ops, SparseCore 0:
  23.7 46.3 reduce-scatter.1
  71.9 34.3 all-gather.11
  110.1 27.9 all-gather.5
  165.7 79.0 all-gather.7
  246.9 79.2 all-gather.9
